TPU v7x, 32 devices: a whole 2x2x4 slice. The times are simulated.
32 devices in a mesh: fs: 16 (over z, y, x), tp: 2 (over core).
Axes of the slice: x: 2, y: 2, z: 4, core: 2. Of those that a mesh axis runs over, the one named last changes fastest.
Arguments:
- tokens: bfloat16 [6144, 2048], P('fs'), may hold values from -6 to 6
- mixer_norm_gain: float32 [2048], replicated, may hold values from 0.1 to 1.9
- outer_gate_weight: bfloat16 [2048, 2048], P('fs', 'tp'), may hold values from -0.125 to 0.125
- inner_gate_weight: bfloat16 [2048, 2048], P('fs', 'tp'), may hold values from -0.125 to 0.125
- value_projection_weight: bfloat16 [2048, 2048], P('fs', 'tp'), may hold values from -0.125 to 0.125
- filter_taps_weight: float32 [3, 2048], replicated, may hold values from -3 to 3
- mixer_output_weight: bfloat16 [2048, 2048], P('tp', 'fs'), may hold values from -0.125 to 0.125
- feedforward_norm_gain: float32 [2048], replicated, may hold values from 0.1 to 1.9
- up_projection_weight: bfloat16 [2048, 8192], P('fs', 'tp'), may hold values from -0.125 to 0.125
- down_projection_weight: bfloat16 [8192, 2048], P('tp', 'fs'), may hold values from -0.0625 to 0.0625
Outputs:
- layer_out: bfloat16 [6144, 2048], P('fs')
All inputs are finite; a program needn't handle non-finite values.
Results may differ from a plain program's by a relative error of at most 0.02.
Values may be sent and summed in bfloat16 or wider, within the bound.
A program may use at most 128 MiB of HBM per device.

v0:
```python
import jax
import jax.numpy as jnp
from jax import lax
from jax.sharding import PartitionSpec as P


def rms_norm(rows, gain):
    floats = rows.astype(jnp.float32)
    scale = lax.rsqrt(jnp.mean(floats * floats, axis=-1, keepdims=True) + 1e-06)
    return (floats * scale * gain).astype(jnp.bfloat16)


def causal_mix(inner_product_rows, taps):
    length = inner_product_rows.shape[0]
    width = taps.shape[0]
    padded = jnp.pad(inner_product_rows, ((width - 1, 0), (0, 0)))
    total = jnp.zeros_like(inner_product_rows)
    for offset in range(width):
        total = total + taps[offset] * padded[offset : offset + length]
    return total


def settle(partial_value):
    rounded = lax.optimization_barrier(partial_value.astype(jnp.bfloat16))
    return rounded.astype(jnp.float32)


def on_device(
    tokens,
    mixer_norm_gain,
    outer_gate_weight,
    inner_gate_weight,
    value_projection_weight,
    filter_taps_weight,
    mixer_output_weight,
    feedforward_norm_gain,
    up_projection_weight,
    down_projection_weight,
):
    index = lax.axis_index("tp")
    local_width = outer_gate_weight.shape[1]
    first_normed_rows = rms_norm(tokens, mixer_norm_gain)
    pieces = (
        lax.all_gather(outer_gate_weight, "fs", axis=0, tiled=True),
        lax.all_gather(inner_gate_weight, "fs", axis=0, tiled=True),
        lax.all_gather(value_projection_weight, "fs", axis=0, tiled=True),
    )
    columns = first_normed_rows
    outer_gate_rows, inner_gate_rows, value_rows = tuple(
        (jnp.dot(columns, piece, preferred_element_type=jnp.float32) for piece in pieces)
    )
    outer_gate_rows = outer_gate_rows.astype(jnp.bfloat16)
    inner_gate_rows = inner_gate_rows.astype(jnp.bfloat16)
    value_rows = value_rows.astype(jnp.bfloat16)
    taps = lax.dynamic_slice_in_dim(filter_taps_weight, index * local_width, local_width, 1)
    inner_product_rows = inner_gate_rows.astype(jnp.float32) * value_rows.astype(jnp.float32)
    mixed = (outer_gate_rows.astype(jnp.float32) * causal_mix(inner_product_rows, taps)).astype(
        jnp.bfloat16
    )
    partial_value = settle(
        jnp.dot(
            mixed,
            lax.all_gather(mixer_output_weight, "fs", axis=1, tiled=True),
            preferred_element_type=jnp.float32,
        )
    )
    total = lax.psum(partial_value.astype(jnp.bfloat16), "tp").astype(jnp.float32)
    resid = (tokens.astype(jnp.float32) + total).astype(jnp.bfloat16)
    second = rms_norm(resid, feedforward_norm_gain)
    columns = second
    lifted = jnp.maximum(
        jnp.dot(
            columns,
            lax.all_gather(up_projection_weight, "fs", axis=0, tiled=True),
            preferred_element_type=jnp.float32,
        ),
        0.0,
    )
    hidden = (lifted * lifted).astype(jnp.bfloat16)
    down = jnp.dot(
        hidden,
        lax.all_gather(down_projection_weight, "fs", axis=1, tiled=True),
        preferred_element_type=jnp.float32,
    )
    total_down = lax.psum(settle(down).astype(jnp.bfloat16), "tp").astype(jnp.float32)
    return (resid.astype(jnp.float32) + total_down).astype(jnp.bfloat16)


def solution(mesh):
    return jax.shard_map(
        on_device,
        mesh=mesh,
        in_specs=(
            P("fs", None),
            P(),
            P("fs", "tp"),
            P("fs", "tp"),
            P("fs", "tp"),
            P(),
            P("tp", "fs"),
            P(),
            P("fs", "tp"),
            P("tp", "fs"),
        ),
        out_specs=P("fs", None),
        check_vma=False,
    )
```

profile of v0, /device:TPU:0, one launch (start us, length us, event | category | flops | bytes accessed | tf_op | source)
XLA Modules:
  0.0 859.7 jit_solution(13592114975854171140)
XLA Ops:
  6.5 0.0 all-gather.9.cloned.1.call-start
  6.5 0.7 all-gather.9.cloned.1.call-update
  7.3 0.0 all-gather.11.cloned.1.call-start
  7.3 0.7 all-gather.11.cloned.1.call-update
  8.0 0.0 all-gather.13.cloned.1.call-start
  8.1 0.7 all-gather.13.cloned.1.call-update
  8.7 0.0 all-gather.7.cloned.1.call-start
  8.8 0.5 all-gather.7.cloned.1.call-update
  9.3 0.0 all-reduce.4.cloned.1.call-start
  9.4 0.9 constant_dynamic-slice_fusion
  10.3 1.8 fusion.1
  12.1 0.0 copy-start
  12.1 0.0 copy-start.2
  12.1 76.3 %all-gather.9.cloned.1.call-done = bf16[2048,1024]{1,0:T(8,128)(2,1)} async-done(((bf16[128,1024]{1,0:T(8,128)(2,1)}), bf16[2048,1024]{1,0:T(8,128)(2,1)}) %all-gather.9.cloned.1.call-update) | async-done | bytes 4194320 | tf_op jit(solution)/shard_map/all_gather | solution.py:45
  88.4 4.5 convolution_convert_fusion.2
  93.0 72.5 %all-gather.11.cloned.1.call-done = bf16[2048,1024]{1,0:T(8,128)(2,1)} async-done(((bf16[128,1024]{1,0:T(8,128)(2,1)}), bf16[2048,1024]{1,0:T(8,128)(2,1)}) %all-gather.11.cloned.1.call-update) | async-done | bytes 4194320 | tf_op jit(solution)/shard_map/all_gather | solution.py:46
  165.4 0.0 copy-done
  165.4 0.0 copy-done.2
  165.4 5.2 convert_multiply_fusion.4
  170.6 84.9 %all-gather.13.cloned.1.call-done = bf16[1024,2048]{1,0:T(8,128)(2,1)} async-done(((bf16[1024,128]{1,0:T(8,128)(2,1)}), bf16[1024,2048]{1,0:T(8,128)(2,1)}) %all-gather.13.cloned.1.call-update) | async-done | bytes 4194320 | tf_op jit(solution)/shard_map/all_gather | solution.py:63
  255.5 76.4 %all-gather.7.cloned.1.call-done = bf16[2048,1024]{1,0:T(8,128)(2,1)} async-done(((bf16[128,1024]{1,0:T(8,128)(2,1)}), bf16[2048,1024]{1,0:T(8,128)(2,1)}) %all-gather.7.cloned.1.call-update) | async-done | bytes 4194320 | tf_op jit(solution)/shard_map/all_gather | solution.py:44
  331.9 9.9 %convolution_convert_fusion = bf16[384,2048]{1,0:T(8,128)(2,1)} fusion(bf16[1024,2048]{1,0:T(8,128)(2,1)} %all-gather.13.cloned.1.call-done, f32[384,1024]{1,0:T(8,128)} %convert_multiply_fusion.4, bf16[2048,1024]{1,0:T(8,128)(2,1)} %all-gather.7.cloned.1.call-done, f32[1024]{0:T(1024)S(1)} %bitcast.11, f32[1024]{0:T(1024)S(1)} %bitcast.10, ...), kind=kOutput, calls=%fused_computation.18 | convolution fusion | flops 3228696576 | bytes 13129216 | tf_op jit(solution)/shard_map/dot_general | solution.py:61
  341.8 0.0 copy-start.3
  341.8 0.0 all-reduce.4.cloned.1.call-update
  341.8 0.0 all-gather.15.cloned.1.call-start
  341.9 0.5 all-gather.15.cloned.1.call-update
  342.4 0.0 all-gather.17.cloned.1.call-start
  342.5 0.7 all-gather.17.cloned.1.call-update
  343.2 0.2 all-reduce.6.cloned.1.call-start
  343.4 17.6 %all-reduce.4.cloned.1.call-done = bf16[384,2048]{1,0:T(8,128)(2,1)} async-done(((bf16[384,2048]{1,0:T(8,128)(2,1)}), bf16[384,2048]{1,0:T(8,128)(2,1)}) %all-reduce.4.cloned.1.call-update) | async-done | bytes 1572880 | tf_op jit(solution)/shard_map/psum | solution.py:67
  361.0 0.0 copy-start.1
  361.0 2.1 fusion.5
  363.1 192.7 %all-gather.15.cloned.1.call-done = bf16[2048,4096]{1,0:T(8,128)(2,1)} async-done(((bf16[128,4096]{1,0:T(8,128)(2,1)}), bf16[2048,4096]{1,0:T(8,128)(2,1)}) %all-gather.15.cloned.1.call-update) | async-done | bytes 16777232 | tf_op jit(solution)/shard_map/all_gather | solution.py:74
  555.8 250.0 %all-gather.17.cloned.1.call-done = bf16[4096,2048]{1,0:T(8,128)(2,1)} async-done(((bf16[4096,128]{1,0:T(8,128)(2,1)}), bf16[4096,2048]{1,0:T(8,128)(2,1)}) %all-gather.17.cloned.1.call-update) | async-done | bytes 16777232 | tf_op jit(solution)/shard_map/all_gather | solution.py:82
  805.8 0.0 copy-done.3
  805.8 0.0 copy-done.1
  805.8 24.9 %fusion.10 = bf16[384,2048]{1,0:T(8,128)(2,1)} fusion(bf16[4096,2048]{1,0:T(8,128)(2,1)} %all-gather.17.cloned.1.call-done, bf16[2048,4096]{1,0:T(8,128)(2,1)} %all-gather.15.cloned.1.call-done, f32[2048]{0:T(1024)S(1)} %copy-done.3, f32[384]{0:T(512)S(1)} %add_rsqrt_fusion, bf16[384,2048]{1,0:T(8,128)(2,1)S(1)} %copy-done, bf16[384,2048]{1,0:T(8,128)(2,1)S(1)} %copy-done.1), kind=kOutput, calls=%fused_computation.17 | convolution fusion | flops 12896698368 | bytes 38282752 | tf_op jit(solution)/shard_map/dot_general | solution.py:80
  830.8 0.0 all-reduce.6.cloned.1.call-update
  830.8 18.7 %all-reduce.6.cloned.1.call-done = bf16[384,2048]{1,0:T(8,128)(2,1)} async-done(((bf16[384,2048]{1,0:T(8,128)(2,1)}), bf16[384,2048]{1,0:T(8,128)(2,1)}) %all-reduce.6.cloned.1.call-update) | async-done | bytes 1572880 | tf_op jit(solution)/shard_map/psum | solution.py:85
  849.5 3.4 fusion.8
  (2 shorter events, 0.0 us)
Async XLA Ops:
  6.5 81.9 %all-gather.9.cloned.1.call-start = ((), (), s32[]{:S(2)}) async-start(), calls=%async_computation.1 | async-start | bytes 4456448 | tf_op jit(solution)/shard_map/all_gather | solution.py:45
  7.3 158.2 %all-gather.11.cloned.1.call-start = ((), (), s32[]{:S(2)}) async-start(), calls=%async_computation.2 | async-start | bytes 4456448 | tf_op jit(solution)/shard_map/all_gather | solution.py:46
  8.0 247.5 %all-gather.13.cloned.1.call-start = ((), (), s32[]{:S(2)}) async-start(), calls=%async_computation.3 | async-start | bytes 4456448 | tf_op jit(solution)/shard_map/all_gather | solution.py:63
  8.7 323.2 %all-gather.7.cloned.1.call-start = ((), (), s32[]{:S(2)}) async-start(), calls=%async_computation | async-start | bytes 4456448 | tf_op jit(solution)/shard_map/all_gather | solution.py:44
  9.3 351.6 %all-reduce.4.cloned.1.call-start = ((), (), s32[]{:S(2)}) async-start(), calls=%async_computation.4 | async-start | bytes 3145728 | tf_op jit(solution)/shard_map/psum | solution.py:67
  12.1 153.3 %copy-start = (bf16[384,2048]{1,0:T(8,128)(2,1)S(1)}, bf16[384,2048]{1,0:T(8,128)(2,1)}, u32[]{:S(2)}) copy-start(bf16[384,2048]{1,0:T(8,128)(2,1)} %param.10) | copy-start | bytes 4718596
  12.1 153.3 %copy-start.2 = (f32[2048]{0:T(1024)S(1)}, f32[2048]{0:T(1024)}, u32[]{:S(2)}) copy-start(f32[2048]{0:T(1024)} %param.11) | copy-start | bytes 24580
  341.8 464.0 %copy-start.3 = (f32[2048]{0:T(1024)S(1)}, f32[2048]{0:T(1024)}, u32[]{:S(2)}) copy-start(f32[2048]{0:T(1024)} %param.17) | copy-start | bytes 24580
  341.8 214.0 %all-gather.15.cloned.1.call-start = ((), (), s32[]{:S(2)}) async-start(), calls=%async_computation.5 | async-start | bytes 17825792 | tf_op jit(solution)/shard_map/all_gather | solution.py:74
  342.4 463.4 %all-gather.17.cloned.1.call-start = ((), (), s32[]{:S(2)}) async-start(), calls=%async_computation.6 | async-start | bytes 17825792 | tf_op jit(solution)/shard_map/all_gather | solution.py:82
  343.2 506.3 %all-reduce.6.cloned.1.call-start = ((), (), s32[]{:S(2)}) async-start(), calls=%async_computation.7 | async-start | bytes 3145728 | tf_op jit(solution)/shard_map/psum | solution.py:85
  361.0 444.9 %copy-start.1 = (bf16[384,2048]{1,0:T(8,128)(2,1)S(1)}, bf16[384,2048]{1,0:T(8,128)(2,1)}, u32[]{:S(2)}) copy-start(bf16[384,2048]{1,0:T(8,128)(2,1)} %all-reduce.4.cloned.1.call-done) | copy-start | bytes 4718596
Sparse Core Ops, SparseCore 0:
  10.1 78.3 all-gather.8
  91.2 74.1 all-gather.10
  168.1 87.3 all-gather.12
  258.1 73.7 all-gather.6
  342.0 18.9 all-reduce.3
  363.6 192.1 all-gather.14
  558.5 247.2 all-gather.16
  830.9 18.5 all-reduce.5
where the time goes:
time: 860 us
  waiting for transfers between devices  793 us (92%)
  matrix products  44.5 us (5%)
  between operations  13.5 us (2%)
    all_gather x1, waiting for transfers between devices, on_device(): lax.all_gather(down_projection_weight, 'fs', axis=1, tiled=True)  250 us
    all_gather x1, waiting for transfers between devices, on_device(): lax.all_gather(up_projection_weight, 'fs', axis=0, tiled=True)  193 us
    all_gather x1, waiting for transfers between devices, on_device(): lax.all_gather(mixer_output_weight, 'fs', axis=1, tiled=True)  84.9 us
    all_gather x1, waiting for transfers between devices, on_device(): lax.all_gather(outer_gate_weight, 'fs', axis=0, tiled=True)  76.4 us
    all_gather x1, waiting for transfers between devices, on_device(): lax.all_gather(inner_gate_weight, 'fs', axis=0, tiled=True)  76.3 us
    all_gather x1, waiting for transfers between devices, on_device(): lax.all_gather(value_projection_weight, 'fs', axis=0, tiled=True)  72.5 us
    dot_general x1, matrix products, on_device(): jnp.dot(hidden, lax.all_gather(down_projection_weight, 'fs', axis=1, tile...  24.9 us
    psum x1, waiting for transfers between devices, on_device(): lax.psum(settle(down).astype(jnp.bfloat16), 'tp').astype(jnp.float32)  18.7 us
  transfers between devices with their start and end apart: 8, of which 8 were waited for; matrix products, arithmetic and copies ran while one was open for 2% of the time, Pallas kernels for 0%

commit v1 on v0

--- a/solution.py
+++ b/solution.py
@@ -79,7 +79,7 @@
     hidden = (lifted * lifted).astype(jnp.bfloat16)
     down = jnp.dot(
         hidden,
-        lax.all_gather(down_projection_weight, "fs", axis=1, tiled=True),
+        jnp.concatenate(lax.all_gather(down_projection_weight, "fs"), 1),
         preferred_element_type=jnp.float32,
     )
     total_down = lax.psum(settle(down).astype(jnp.bfloat16), "tp").astype(jnp.float32)

time: 860 us -> 796 us (0.926)
  waiting for transfers between devices: 793 us -> 714 us
  local copies, waits for them, and re-layouts: 0.93 us -> 22.6 us
    all_gather x1, waiting for transfers between devices: 250 us -> 193 us  [on_device(): lax.all_gather(down_projection_weight, 'fs')]
    all_gather x1, waiting for transfers between devices: 193 us -> 170 us  [on_device(): lax.all_gather(up_projection_weight, 'fs', axis=0, tiled=True)]
    reshape x0 -> x1, local copies, waits for them, and re-layouts: none -> 21.6 us  [on_device(): jnp.concatenate(lax.all_gather(down_projection_weight, 'fs'), 1)]
  transfers between devices with their start and end apart: 8 -> 8, of which waited for: 8 -> 8; matrix products, arithmetic and copies ran while one was open for 2% -> 5% of each run, Pallas kernels for 0% -> 0%
where the time goes in v1:
time: 796 us; the launch traced here: 795 us
  waiting for transfers between devices  714 us (90%)
  matrix products  38.3 us (5%)
  local copies, waits for them, and re-layouts  22.6 us (3%)
  between operations  13.5 us (2%)
    all_gather x1, waiting for transfers between devices, on_device(): lax.all_gather(down_projection_weight, 'fs')  193 us
    all_gather x1, waiting for transfers between devices, on_device(): lax.all_gather(up_projection_weight, 'fs', axis=0, tiled=True)  170 us
    all_gather x1, waiting for transfers between devices, on_device(): lax.all_gather(mixer_output_weight, 'fs', axis=1, tiled=True)  84.9 us
    all_gather x1, waiting for transfers between devices, on_device(): lax.all_gather(outer_gate_weight, 'fs', axis=0, tiled=True)  76.4 us
    all_gather x1, waiting for transfers between devices, on_device(): lax.all_gather(inner_gate_weight, 'fs', axis=0, tiled=True)  76.3 us
    all_gather x1, waiting for transfers between devices, on_device(): lax.all_gather(value_projection_weight, 'fs', axis=0, tiled=True)  72.5 us
    reshape x1, local copies, waits for them, and re-layouts, on_device(): jnp.concatenate(lax.all_gather(down_projection_weight, 'fs'), 1)  21.6 us
    dot_general x1, matrix products, on_device(): jnp.dot(hidden, jnp.concatenate(lax.all_gather(down_projection_weight, 'f...  18.8 us
  transfers between devices with their start and end apart: 8, of which 8 were waited for; matrix products, arithmetic and copies ran while one was open for 5% of the time, Pallas kernels for 0%

profile of v1, /device:TPU:0, one launch (start us, length us, event | category | flops | bytes accessed | tf_op | source)
XLA Modules:
  0.0 795.4 jit_solution(6992488844029469271)
XLA Ops:
  6.5 0.0 all-gather.10.cloned.1.call-start
  6.5 0.7 all-gather.10.cloned.1.call-update
  7.3 0.0 all-gather.12.cloned.1.call-start
  7.3 0.7 all-gather.12.cloned.1.call-update
  8.0 0.0 all-gather.14.cloned.1.call-start
  8.1 0.7 all-gather.14.cloned.1.call-update
  8.7 0.0 all-gather.8.cloned.1.call-start
  8.8 0.5 all-gather.8.cloned.1.call-update
  9.3 0.0 all-reduce.4.cloned.1.call-start
  9.4 0.9 constant_dynamic-slice_fusion
  10.3 1.8 fusion
  12.1 0.0 copy-start
  12.1 0.0 copy-start.2
  12.1 76.3 %all-gather.10.cloned.1.call-done = bf16[2048,1024]{1,0:T(8,128)(2,1)} async-done(((bf16[128,1024]{1,0:T(8,128)(2,1)}), bf16[2048,1024]{1,0:T(8,128)(2,1)}) %all-gather.10.cloned.1.call-update) | async-done | bytes 4194320 | tf_op jit(solution)/shard_map/all_gather | solution.py:45
  88.4 4.5 convolution_convert_fusion.2
  93.0 72.5 %all-gather.12.cloned.1.call-done = bf16[2048,1024]{1,0:T(8,128)(2,1)} async-done(((bf16[128,1024]{1,0:T(8,128)(2,1)}), bf16[2048,1024]{1,0:T(8,128)(2,1)}) %all-gather.12.cloned.1.call-update) | async-done | bytes 4194320 | tf_op jit(solution)/shard_map/all_gather | solution.py:46
  165.4 0.0 copy-done
  165.4 0.0 copy-done.2
  165.4 5.2 convert_multiply_fusion.4
  170.6 84.9 %all-gather.14.cloned.1.call-done = bf16[1024,2048]{1,0:T(8,128)(2,1)} async-done(((bf16[1024,128]{1,0:T(8,128)(2,1)}), bf16[1024,2048]{1,0:T(8,128)(2,1)}) %all-gather.14.cloned.1.call-update) | async-done | bytes 4194320 | tf_op jit(solution)/shard_map/all_gather | solution.py:63
  255.5 76.4 %all-gather.8.cloned.1.call-done = bf16[2048,1024]{1,0:T(8,128)(2,1)} async-done(((bf16[128,1024]{1,0:T(8,128)(2,1)}), bf16[2048,1024]{1,0:T(8,128)(2,1)}) %all-gather.8.cloned.1.call-update) | async-done | bytes 4194320 | tf_op jit(solution)/shard_map/all_gather | solution.py:44
  331.9 9.8 %convolution_convert_fusion = bf16[384,2048]{1,0:T(8,128)(2,1)} fusion(bf16[1024,2048]{1,0:T(8,128)(2,1)} %all-gather.14.cloned.1.call-done, f32[384,1024]{1,0:T(8,128)} %convert_multiply_fusion.4, bf16[2048,1024]{1,0:T(8,128)(2,1)} %all-gather.8.cloned.1.call-done, f32[1024]{0:T(1024)S(1)} %bitcast.17, f32[1024]{0:T(1024)S(1)} %bitcast.16, ...), kind=kOutput, calls=%fused_computation.17 | convolution fusion | flops 3228696576 | bytes 13129216 | tf_op jit(solution)/shard_map/dot_general | solution.py:61
  341.7 0.0 all-reduce.4.cloned.1.call-update
  341.8 0.0 all-gather.18.cloned.1.call-start
  341.8 0.5 all-gather.18.cloned.1.call-update
  342.3 0.0 all-gather.16.cloned.1.call-start
  342.4 0.7 all-gather.16.cloned.1.call-update
  343.1 0.0 all-reduce.6.cloned.1.call-start
  343.1 17.7 %all-reduce.4.cloned.1.call-done = bf16[384,2048]{1,0:T(8,128)(2,1)} async-done(((bf16[384,2048]{1,0:T(8,128)(2,1)}), bf16[384,2048]{1,0:T(8,128)(2,1)}) %all-reduce.4.cloned.1.call-update) | async-done | bytes 1572880 | tf_op jit(solution)/shard_map/psum | solution.py:67
  360.9 2.0 fusion.4
  362.9 192.8 %all-gather.18.cloned.1.call-done = bf16[65536,128]{1,0:T(8,128)(2,1)} async-done(((bf16[4096,128]{1,0:T(8,128)(2,1)}), bf16[65536,128]{1,0:T(8,128)(2,1)}) %all-gather.18.cloned.1.call-update) | async-done | bytes 16777232 | tf_op jit(solution)/shard_map/all_gather | solution.py:82
  555.7 0.0 copy-start.1
  555.7 0.0 copy-start.3
  555.7 21.6 %copy.11 = bf16[4096,16,128]{0,2,1:T(8,128)(2,1)} copy(bf16[4096,16,128]{2,0,1:T(8,128)(2,1)} %bitcast.13) | data formatting | bytes 33554432 | tf_op jit(solution)/shard_map/reshape | solution.py:82
  577.4 170.3 %all-gather.16.cloned.1.call-done = bf16[2048,4096]{1,0:T(8,128)(2,1)} async-done(((bf16[128,4096]{1,0:T(8,128)(2,1)}), bf16[2048,4096]{1,0:T(8,128)(2,1)}) %all-gather.16.cloned.1.call-update) | async-done | bytes 16777232 | tf_op jit(solution)/shard_map/all_gather | solution.py:74
  747.7 0.0 copy-done.1
  747.7 0.0 copy-done.3
  747.7 18.8 %fusion.9 = bf16[384,2048]{1,0:T(8,128)(2,1)} fusion(bf16[4096,2048]{0,1:T(8,128)(2,1)} %bitcast.14, bf16[2048,4096]{1,0:T(8,128)(2,1)} %all-gather.16.cloned.1.call-done, f32[2048]{0:T(1024)S(1)} %copy-done.3, f32[384]{0:T(512)S(1)} %add_rsqrt_fusion, bf16[384,2048]{1,0:T(8,128)(2,1)S(1)} %copy-done, bf16[384,2048]{1,0:T(8,128)(2,1)S(1)} %copy-done.1), kind=kOutput, calls=%fused_computation.16 | convolution fusion | flops 12896698368 | bytes 38282752 | tf_op jit(solution)/shard_map/dot_general | solution.py:80
  766.5 0.0 all-reduce.6.cloned.1.call-update
  766.5 18.7 %all-reduce.6.cloned.1.call-done = bf16[384,2048]{1,0:T(8,128)(2,1)} async-done(((bf16[384,2048]{1,0:T(8,128)(2,1)}), bf16[384,2048]{1,0:T(8,128)(2,1)}) %all-reduce.6.cloned.1.call-update) | async-done | bytes 1572880 | tf_op jit(solution)/shard_map/psum | solution.py:85
  785.2 3.4 fusion.7
  (2 shorter events, 0.0 us)
Async XLA Ops:
  6.5 81.9 %all-gather.10.cloned.1.call-start = ((), (), s32[]{:S(2)}) async-start(), calls=%async_computation.1 | async-start | bytes 4456448 | tf_op jit(solution)/shard_map/all_gather | solution.py:45
  7.3 158.2 %all-gather.12.cloned.1.call-start = ((), (), s32[]{:S(2)}) async-start(), calls=%async_computation.2 | async-start | bytes 4456448 | tf_op jit(solution)/shard_map/all_gather | solution.py:46
  8.0 247.5 %all-gather.14.cloned.1.call-start = ((), (), s32[]{:S(2)}) async-start(), calls=%async_computation.3 | async-start | bytes 4456448 | tf_op jit(solution)/shard_map/all_gather | solution.py:63
  8.7 323.2 %all-gather.8.cloned.1.call-start = ((), (), s32[]{:S(2)}) async-start(), calls=%async_computation | async-start | bytes 4456448 | tf_op jit(solution)/shard_map/all_gather | solution.py:44
  9.3 351.6 %all-reduce.4.cloned.1.call-start = ((), (), s32[]{:S(2)}) async-start(), calls=%async_computation.4 | async-start | bytes 3145728 | tf_op jit(solution)/shard_map/psum | solution.py:67
  12.1 153.3 %copy-start = (bf16[384,2048]{1,0:T(8,128)(2,1)S(1)}, bf16[384,2048]{1,0:T(8,128)(2,1)}, u32[]{:S(2)}) copy-start(bf16[384,2048]{1,0:T(8,128)(2,1)} %param.10) | copy-start | bytes 4718596
  12.1 153.3 %copy-start.2 = (f32[2048]{0:T(1024)S(1)}, f32[2048]{0:T(1024)}, u32[]{:S(2)}) copy-start(f32[2048]{0:T(1024)} %param.11) | copy-start | bytes 24580
  341.8 213.9 %all-gather.18.cloned.1.call-start = ((), (), s32[]{:S(2)}) async-start(), calls=%async_computation.7 | async-start | bytes 17825792 | tf_op jit(solution)/shard_map/all_gather | solution.py:82
  342.3 405.4 %all-gather.16.cloned.1.call-start = ((), (), s32[]{:S(2)}) async-start(), calls=%async_computation.5 | async-start | bytes 17825792 | tf_op jit(solution)/shard_map/all_gather | solution.py:74
  343.1 442.1 %all-reduce.6.cloned.1.call-start = ((), (), s32[]{:S(2)}) async-start(), calls=%async_computation.6 | async-start | bytes 3145728 | tf_op jit(solution)/shard_map/psum | solution.py:85
  555.7 192.0 %copy-start.1 = (bf16[384,2048]{1,0:T(8,128)(2,1)S(1)}, bf16[384,2048]{1,0:T(8,128)(2,1)}, u32[]{:S(2)}) copy-start(bf16[384,2048]{1,0:T(8,128)(2,1)} %all-reduce.4.cloned.1.call-done) | copy-start | bytes 4718596
  555.7 192.0 %copy-start.3 = (f32[2048]{0:T(1024)S(1)}, f32[2048]{0:T(1024)}, u32[]{:S(2)}) copy-start(f32[2048]{0:T(1024)} %param.17) | copy-start | bytes 24580
Sparse Core Ops, SparseCore 0:
  10.1 78.3 all-gather.9
  91.2 74.1 all-gather.11
  168.1 87.3 all-gather.13
  258.1 73.7 all-gather.7
  341.9 18.9 all-reduce.3
  363.5 192.1 all-gather.17
  558.5 189.1 all-gather.15
  766.6 18.5 all-reduce.5
